TPU v7x, 32 devices: a whole 2x2x4 slice. The times are simulated.
32 devices in a mesh: sp: 8 (over z, x), tp: 4 (over y, core).
Axes of the slice: x: 2, y: 2, z: 4, core: 2. Of those that a mesh axis runs over, the one named last changes fastest.
Arguments:
- residual: bfloat16 [2048, 2048], P(('sp', 'tp')), may hold values from -6 to 6
- query_wide: bfloat16 [2048, 512], P('sp', 'tp'), may hold values from -8 to 8
- key_wide: bfloat16 [2048, 512], P('sp', 'tp'), may hold values from -8 to 8
- value_wide: bfloat16 [2048, 512], P('sp', 'tp'), may hold values from -6 to 6
- query_narrow: bfloat16 [2048, 512], P('sp', 'tp'), may hold values from -8 to 8
- key_narrow: bfloat16 [2048, 512], P('sp', 'tp'), may hold values from -8 to 8
- value_narrow: bfloat16 [2048, 512], P('sp', 'tp'), may hold values from -6 to 6
- gate_wide: float32 [2048, 4], P('sp', 'tp'), may hold values from -2 to 20
- gate_narrow: float32 [2048, 8], P('sp', 'tp'), may hold values from -2 to 20
- out_wide: bfloat16 [512, 2048], replicated, may hold values from -0.1875 to 0.1875
- out_narrow: bfloat16 [512, 2048], replicated, may hold values from -0.1875 to 0.1875
- norm_gain: float32 [2048], replicated, may hold values from 0.1 to 1.9
- routing: int32 [2048, 2], P(('sp', 'tp')), may hold values from 0 to 7, as said below
- route_weight: float32 [2048, 2], P(('sp', 'tp')), may hold values from 0.3 to 1.5
- gate_weight: bfloat16 [8, 2048, 1024], P('sp', None, 'tp'), may hold values from -0.125 to 0.125
- up_weight: bfloat16 [8, 2048, 1024], P('sp', None, 'tp'), may hold values from -0.125 to 0.125
- down_weight: bfloat16 [8, 1024, 2048], P('sp', 'tp'), may hold values from -0.1875 to 0.1875
Outputs:
- result: bfloat16 [2048, 2048], P(('sp', 'tp'))
Inputs may be any that keep to these rules, and one draw needn't show every extreme that they name: `routing`: each row names 2 different experts of one group (experts g * 2 to g * 2 + 1). In each aligned block of 64 rows (the rows of one device) no expert is named by more than 32 rows; one group, the same for all blocks, has each of its experts named by exactly 32 rows of every block.
All inputs are finite; a program needn't handle non-finite values.
Results may differ from a plain program's by a relative error of at most 0.017.
Values may be sent and summed in bfloat16 or wider, within the bound.
A program may use at most 128 MiB of HBM per device.

v0:
```python
import math

import jax
import jax.numpy as jnp
from jax import lax
from jax.sharding import PartitionSpec as P

HW = 128
HN = 64
GROUPS = 4


epsilon = 1e-06


def globalize(pieces, shard_rows):
    shards = pieces.shape[0] // shard_rows
    grid = pieces.reshape(shards, shard_rows, pieces.shape[1])
    endings = grid[:, -1, :]
    offsets = jnp.cumsum(endings, axis=0) - endings
    return (grid + offsets[:, None, :]).reshape(pieces.shape)


def head_block(
    state, queries, query_decay, keys, values, key_decay, first_key, first_query, head_width
):
    highest_old, weight_sum, weighted = state
    query_rows = queries.shape[0]
    head_count = query_decay.shape[1]
    key_rows = keys.shape[0]
    grid_query = queries.reshape(query_rows, head_count, head_width)
    grid_key = keys.reshape(key_rows, head_count, head_width)
    grid_value = values.reshape(key_rows, head_count, head_width)
    scores = jnp.einsum("thd,phd->htp", grid_query, grid_key, preferred_element_type=jnp.float32)
    scores = scores * head_width ** (-0.5) + query_decay.T[:, :, None] - key_decay.T[:, None, :]
    query_place = first_query + jnp.arange(query_rows, dtype=jnp.int32)
    key_place = first_key + jnp.arange(key_rows, dtype=jnp.int32)
    scores = jnp.where(key_place[None, None, :] <= query_place[None, :, None], scores, -jnp.inf)
    highest = jnp.maximum(highest_old, jnp.max(scores, axis=2))
    weights = jnp.exp(scores - highest[:, :, None])
    shrink = jnp.exp(highest_old - highest)
    weight_sum = weight_sum * shrink + jnp.sum(weights, axis=2)
    product = jnp.einsum(
        "htp,phd->htd", weights.astype(jnp.bfloat16), grid_value, preferred_element_type=jnp.float32
    )
    weighted = weighted * shrink[:, :, None] + product
    return (highest, weight_sum, weighted)


def fresh_state(head_count, shard_rows, head_width):
    return (
        jnp.full((head_count, shard_rows), -1e30, jnp.float32),
        jnp.zeros((head_count, shard_rows), jnp.float32),
        jnp.zeros((head_count, shard_rows, head_width), jnp.float32),
    )


def finish(state, shard_rows):
    highest, weight_sum, weighted = state
    mixed_heads = weighted / weight_sum[:, :, None]
    joined = jnp.transpose(mixed_heads, (1, 0, 2))
    return joined.reshape(shard_rows, weighted.shape[0] * weighted.shape[2]).astype(jnp.bfloat16)


def body(
    residual,
    query_wide,
    key_wide,
    value_wide,
    query_narrow,
    key_narrow,
    value_narrow,
    gate_wide,
    gate_narrow,
    out_wide,
    out_narrow,
    norm_gain,
    routing,
    route_weight,
    gate_weight,
    up_weight,
    down_weight,
):
    shard_rows = query_wide.shape[0]
    half_rows = shard_rows // 2
    sp_place = lax.axis_index("sp")
    first_query = sp_place * shard_rows
    running_wide = jnp.cumsum(jax.nn.log_sigmoid(gate_wide), axis=0)
    running_narrow = jnp.cumsum(jax.nn.log_sigmoid(gate_narrow), axis=0)
    pieces_wide, pieces_narrow = (
        lax.all_gather(running_wide, "sp", axis=0, tiled=True),
        lax.all_gather(running_narrow, "sp", axis=0, tiled=True),
    )
    every_wide = globalize(pieces_wide, shard_rows)
    every_narrow = globalize(pieces_narrow, shard_rows)
    late_first = first_query + half_rows
    halves = []
    for place, part_wide, part_narrow in (
        (first_query, query_wide[:half_rows], query_narrow[:half_rows]),
        (late_first, query_wide[half_rows:], query_narrow[half_rows:]),
    ):
        halves.append(
            (
                place,
                part_wide,
                part_narrow,
                lax.dynamic_slice_in_dim(every_wide, place, half_rows, 0),
                lax.dynamic_slice_in_dim(every_narrow, place, half_rows, 0),
            )
        )

    def half_state():
        return (
            fresh_state(gate_wide.shape[1], half_rows, HW),
            fresh_state(gate_narrow.shape[1], half_rows, HN),
        )

    state = (half_state(), half_state())
    keys_wide = lax.all_gather(key_wide, "sp", axis=0, tiled=True)
    values_wide = lax.all_gather(value_wide, "sp", axis=0, tiled=True)
    keys_narrow = lax.all_gather(key_narrow, "sp", axis=0, tiled=True)
    values_narrow = lax.all_gather(value_narrow, "sp", axis=0, tiled=True)
    span_rows = keys_wide.shape[0]
    block_size = math.gcd(span_rows, 2048)

    def visit(carried, position):
        inside = position * block_size

        def take_block(source):
            return lax.dynamic_slice_in_dim(source, inside, block_size, 0)

        def take_decay(source):
            return lax.dynamic_slice_in_dim(source, inside, block_size, 0)

        block_kw = take_block(keys_wide)
        block_vw = take_block(values_wide)
        block_kn = take_block(keys_narrow)
        block_vn = take_block(values_narrow)
        block_dw = take_decay(every_wide)
        block_dn = take_decay(every_narrow)

        def one_half(current, half):
            place, part_wide, part_narrow, query_decay_wide, query_decay_narrow = half

            def work(inner):
                first = head_block(
                    inner[0],
                    part_wide,
                    query_decay_wide,
                    block_kw,
                    block_vw,
                    block_dw,
                    inside,
                    place,
                    HW,
                )
                second = head_block(
                    inner[1],
                    part_narrow,
                    query_decay_narrow,
                    block_kn,
                    block_vn,
                    block_dn,
                    inside,
                    place,
                    HN,
                )
                return (first, second)

            def skip(inner):
                return inner

            return lax.cond(inside <= place + half_rows - 1, work, skip, current)

        updated = (one_half(carried[0], halves[0]), one_half(carried[1], halves[1]))
        return (updated, None)

    state, _ = lax.scan(visit, state, jnp.arange(span_rows // block_size, dtype=jnp.int32))
    att_wide = jnp.concatenate(
        [finish(state[0][0], half_rows), finish(state[1][0], half_rows)], axis=0
    )
    att_narrow = jnp.concatenate(
        [finish(state[0][1], half_rows), finish(state[1][1], half_rows)], axis=0
    )
    own_rows = residual.shape[0]
    tp_place = lax.axis_index("tp")
    rows_wide = lax.dynamic_slice_in_dim(
        out_wide, tp_place * att_wide.shape[1], att_wide.shape[1], 0
    )
    rows_narrow = lax.dynamic_slice_in_dim(
        out_narrow, tp_place * att_narrow.shape[1], att_narrow.shape[1], 0
    )
    first = jnp.dot(att_wide, rows_wide, preferred_element_type=jnp.float32)
    second = jnp.dot(att_narrow, rows_narrow, preferred_element_type=jnp.float32)
    mixed = lax.psum_scatter(
        (first + second).astype(jnp.bfloat16), "tp", scatter_dimension=0, tiled=True
    ).astype(jnp.float32)
    middle = (residual.astype(jnp.float32) + mixed).astype(jnp.bfloat16)
    middle_wide = middle.astype(jnp.float32)
    spread = jnp.mean(middle_wide * middle_wide, axis=1, keepdims=True)
    normed = (middle_wide * lax.rsqrt(spread + epsilon) * norm_gain).astype(jnp.bfloat16)
    features = normed.shape[1]
    chosen_count = routing.shape[1]
    expert_count = gate_weight.shape[0] * lax.axis_size("sp")
    capacity = own_rows * GROUPS // expert_count
    flat_routes = routing.reshape(-1)
    matches = (flat_routes[:, None] == jnp.arange(expert_count, dtype=jnp.int32)[None, :]).astype(
        jnp.int32
    )
    ranking = jnp.sum((jnp.cumsum(matches, axis=0) - matches) * matches, axis=1)
    placing = flat_routes * capacity + ranking
    picker = (
        placing[None, :] == jnp.arange(expert_count * capacity, dtype=jnp.int32)[:, None]
    ).astype(jnp.bfloat16)
    picker = jnp.sum(picker.reshape(expert_count * capacity, own_rows, chosen_count), axis=2)
    outgoing = jnp.dot(picker, normed, preferred_element_type=jnp.float32).astype(jnp.bfloat16)
    outgoing = outgoing.reshape(expert_count, capacity, features)
    arrived = lax.all_to_all(outgoing, "sp", split_axis=0, concat_axis=0, tiled=True)
    pooled = lax.all_gather(arrived.reshape(-1, features), "tp", axis=0, tiled=True)
    gate_value = jnp.dot(pooled, gate_weight[0], preferred_element_type=jnp.float32)
    up_value = jnp.dot(pooled, up_weight[0], preferred_element_type=jnp.float32)
    hidden = (jax.nn.silu(gate_value) * up_value).astype(jnp.bfloat16)
    answers = lax.psum_scatter(
        jnp.dot(hidden, down_weight[0], preferred_element_type=jnp.float32).astype(jnp.bfloat16),
        "tp",
        scatter_dimension=0,
        tiled=True,
    )
    returned = lax.all_to_all(
        answers.reshape(expert_count, capacity, features),
        "sp",
        split_axis=0,
        concat_axis=0,
        tiled=True,
    )
    picked = jnp.take(returned.reshape(expert_count * capacity, features), placing, axis=0)
    picked = picked.reshape(own_rows, chosen_count, features).astype(jnp.float32)
    combined = jnp.sum(route_weight[:, :, None] * picked, axis=1)
    return (middle_wide + combined).astype(jnp.bfloat16)


def solution(mesh):
    placed = (
        P(("sp", "tp"), None),
        P("sp", "tp"),
        P("sp", "tp"),
        P("sp", "tp"),
        P("sp", "tp"),
        P("sp", "tp"),
        P("sp", "tp"),
        P("sp", "tp"),
        P("sp", "tp"),
        P(),
        P(),
        P(),
        P(("sp", "tp"), None),
        P(("sp", "tp"), None),
        P("sp", None, "tp"),
        P("sp", None, "tp"),
        P("sp", "tp", None),
    )
    return jax.shard_map(
        body, mesh=mesh, in_specs=placed, out_specs=P(("sp", "tp"), None), check_vma=False
    )
```

profile of v0, /device:TPU:0, one launch (start us, length us, event | category | flops | bytes accessed | tf_op | source)
XLA Modules:
  0.0 408.9 jit_solution(1248506105477989104)
XLA Ops:
  6.5 0.9 fusion.73
  7.4 0.6 reduce-window.16
  8.5 27.9 %all_gather.25 = f32[2048,2]{0,1:T(2,128)S(1)} all-gather(f32[256,2]{0,1:T(2,128)S(1)} %bitcast.168), channel_id=1, replica_groups=mesh['sp'=8,'tp'=4] {'sp'}, dimensions={0}, use_global_device_ids=true | all-gather | bytes 18432 | tf_op jit(solution)/shard_map/all_gather | solution.py:92
  36.9 0.7 fusion.74
  37.6 0.3 reduce-window.14
  37.9 0.2 slice_reduce_fusion.1
  38.3 19.0 %all_gather.22 = f32[2048,1]{0,1:T(1,128)S(1)} all-gather(f32[256,1]{0,1:T(1,128)S(1)} %reduce_window_sum.69), channel_id=1, replica_groups=mesh['sp'=8,'tp'=4] {'sp'}, dimensions={0}, use_global_device_ids=true | all-gather | bytes 9216 | tf_op jit(solution)/shard_map/all_gather | solution.py:91
  57.7 0.6 add.295
  58.3 0.9 copy.47
  59.3 33.5 %all_gather.24 = bf16[2048,128]{0,1:T(8,128)(2,1)} all-gather(bf16[256,128]{0,1:T(8,128)(2,1)S(1)} %copy.47), channel_id=1, replica_groups=mesh['sp'=8,'tp'=4] {'sp'}, dimensions={0}, use_global_device_ids=true | all-gather | bytes 589824 | tf_op jit(solution)/shard_map/all_gather | solution.py:121
  92.8 0.9 copy.49
  93.7 31.4 %all_gather.26 = bf16[2048,128]{0,1:T(8,128)(2,1)S(1)} all-gather(bf16[256,128]{0,1:T(8,128)(2,1)S(1)} %copy.49), channel_id=1, replica_groups=mesh['sp'=8,'tp'=4] {'sp'}, dimensions={0}, use_global_device_ids=true | all-gather | bytes 589824 | tf_op jit(solution)/shard_map/all_gather | solution.py:122
  125.1 33.7 %all_gather.21 = bf16[2048,128]{1,0:T(8,128)(2,1)} all-gather(bf16[256,128]{1,0:T(8,128)(2,1)} %param.23), channel_id=1, replica_groups=mesh['sp'=8,'tp'=4] {'sp'}, dimensions={0}, use_global_device_ids=true | all-gather | bytes 589824 | tf_op jit(solution)/shard_map/all_gather | solution.py:119
  158.9 31.2 %all_gather.23 = bf16[2048,128]{1,0:T(8,128)(2,1)S(1)} all-gather(bf16[256,128]{1,0:T(8,128)(2,1)S(1)} %copy-done.5), channel_id=1, replica_groups=mesh['sp'=8,'tp'=4] {'sp'}, dimensions={0}, use_global_device_ids=true | all-gather | bytes 589824 | tf_op jit(solution)/shard_map/all_gather | solution.py:120
  190.0 0.6 broadcast.260
  190.6 0.5 broadcast.258
  191.2 0.6 broadcast.265
  191.7 0.5 broadcast.263
  192.3 10.5 %conditional.3 = (f32[1,128]{1,0:T(1,128)S(1)}, f32[1,128,128]{2,1,0:T(8,128)S(1)}, f32[2,128]{1,0:T(2,128)}, f32[2,128,64]{1,2,0:T(8,128)}) conditional(s32[]{:T(128)} %convert_element_type.106, (f32[1,128]{1,0:T(1,128)}, f32[1,128,128]{2,1,0:T(8,128)S(1)}, f32[2,128]{1,0:T(2,128)}, f32[2,128,64]{1,2,0:T(8,128)S(1)}) %tuple.35, (s32[]{:T(128)}, ...), branch_computations={%region_12.13_spmd, %region_13.18_spmd.clone} | conditional | flops 276104320 | bytes 15037726 | solution.py:173
  192.3 0.7 dynamic-slice_bitcast_fusion.1
  192.9 0.6 copy-done.15
  193.5 0.2 iota_compare_fusion.1
  193.7 1.6 copy.51
  195.3 0.8 slice.51
  196.1 1.9 fusion.86
  198.0 0.4 fusion.26
  198.4 1.3 multiply_add_fusion.1
  199.7 1.2 convolution_add_fusion.1
  201.0 0.5 fusion.85
  201.5 0.4 fusion.27
  201.8 0.3 fusion.31
  202.1 0.6 bitcast_add_fusion.1
  202.8 0.5 copy-done.17
  203.3 8.7 %conditional.2 = ((f32[1,128]{1,0:T(1,128)}, f32[1,128,128]{2,1,0:T(8,128)S(1)}, f32[2,128]{1,0:T(2,128)}, f32[2,128,64]{1,2,0:T(8,128)S(1)})) conditional(s32[]{:T(128)} %convert_element_type.103, (f32[1,128]{1,0:T(1,128)}, f32[1,128,128]{2,1,0:T(8,128)S(1)}, f32[2,128]{1,0:T(2,128)}, f32[2,128,64]{1,2,0:T(8,128)S(1)}) %tuple.35, (s32[]{:T(128)}, ...), branch_computations={%region_6.7_spmd, %region_7.12_spmd.clone} | conditional | flops 276104320 | bytes 15033570 | solution.py:173
  203.4 0.9 iota_compare_fusion
  204.3 0.9 copy.50
  205.2 1.9 fusion.84
  207.2 0.4 fusion.7
  207.7 1.3 multiply_add_fusion
  208.9 0.6 convolution_add_fusion
  209.6 0.5 fusion.83
  210.1 0.4 fusion.8
  210.5 0.3 fusion.12
  210.8 1.2 bitcast_add_fusion
  211.9 0.7 divide_convert_fusion.1
  212.6 0.9 divide_convert_fusion
  213.5 0.7 fusion.70
  214.2 0.4 fusion.56
  214.7 2.5 fusion.38
  218.3 21.2 %reduce-scatter.3.cloned.1.call-done = bf16[64,2048]{1,0:T(8,128)(2,1)} async-done(((bf16[256,2048]{1,0:T(8,128)(2,1)}), bf16[64,2048]{1,0:T(8,128)(2,1)}) %reduce-scatter.3.cloned.1.call-update) | async-done | bytes 262160 | tf_op jit(solution)/shard_map/reduce_scatter | solution.py:195
  239.5 1.1 fusion.50
  240.7 1.4 convolution_convert_fusion.1
  242.2 31.1 %all_to_all.10 = bf16[8,32,2048]{2,1,0:T(8,128)(2,1)} all-to-all(bf16[8,32,2048]{2,1,0:T(8,128)(2,1)S(1)} %bitcast.150), channel_id=1, replica_groups=mesh['sp'=8,'tp'=4] {'sp'}, dimensions={0} | all-to-all | bytes 2097152 | tf_op jit(solution)/shard_map/all_to_all | solution.py:218
  273.3 0.2 reduce-scatter.5.cloned.1.call-start
  273.6 32.5 %all-gather.2.cloned.1.call-done = bf16[1024,2048]{1,0:T(8,128)(2,1)} async-done(((bf16[256,2048]{1,0:T(8,128)(2,1)}), bf16[1024,2048]{1,0:T(8,128)(2,1)}) %all-gather.2.cloned.1.call-update) | async-done | bytes 4194320 | tf_op jit(solution)/shard_map/all_gather | solution.py:219
  306.0 4.5 %fusion.43 = f32[1024,256]{1,0:T(8,128)} fusion(bf16[1024,2048]{1,0:T(8,128)(2,1)} %all-gather.2.cloned.1.call-done, bf16[1,2048,256]{2,1,0:T(8,128)(2,1)S(1)} %copy-done.18), kind=kOutput, calls=%fused_computation.73 | convolution fusion | flops 1073741824 | bytes 6291456 | tf_op jit(solution)/shard_map/dot_general | solution.py:220
  310.5 9.4 %convolution_convert_fusion = bf16[1024,2048]{1,0:T(8,128)(2,1)} fusion(bf16[1024,2048]{1,0:T(8,128)(2,1)} %all-gather.2.cloned.1.call-done, bf16[1,256,2048]{2,1,0:T(8,128)(2,1)} %param.37, bf16[1,2048,256]{2,1,0:T(8,128)(2,1)} %param.36, f32[1024,256]{1,0:T(8,128)} %fusion.43), kind=kOutput, calls=%fused_computation.65 | convolution fusion | flops 2151153664 | bytes 11534336 | tf_op jit(solution)/shard_map/dot_general | solution.py:224
  320.0 44.7 %reduce-scatter.5.cloned.1.call-done = bf16[256,2048]{1,0:T(8,128)(2,1)} async-done(((bf16[1024,2048]{1,0:T(8,128)(2,1)}), bf16[256,2048]{1,0:T(8,128)(2,1)}) %reduce-scatter.5.cloned.1.call-update) | async-done | bytes 1048592 | tf_op jit(solution)/shard_map/reduce_scatter | solution.py:223
  364.7 5.5 %all-to-all-start.1 = ((bf16[8,32,2048]{2,1,0:T(8,128)(2,1)}), bf16[8,32,2048]{2,1,0:T(8,128)(2,1)S(1)}, u32[]{:S(2)}, u32[]{:S(2)}) async-start(bf16[8,32,2048]{2,1,0:T(8,128)(2,1)} %bitcast.151), calls=%async_computation.3 | async-start | bytes 2097152 | tf_op jit(solution)/shard_map/all_to_all | solution.py:229
  370.7 25.2 %all-to-all-done.1 = bf16[8,32,2048]{2,1,0:T(8,128)(2,1)S(1)} async-done(((bf16[8,32,2048]{2,1,0:T(8,128)(2,1)}), bf16[8,32,2048]{2,1,0:T(8,128)(2,1)S(1)}, u32[]{:S(2)}, u32[]{:S(2)}) %all-to-all-start.1) | async-done | bytes 1048608 | tf_op jit(solution)/shard_map/all_to_all | solution.py:229
  395.9 1.7 gather_fusion
  397.6 1.4 gather.7
  399.0 2.5 multiply_reduce_fusion
  401.6 0.8 fusion.53
  (98 shorter events, 3.5 us)
Async XLA Ops:
  6.5 207.7 %copy-start = (bf16[512,2048]{1,0:T(8,128)(2,1)S(1)}, bf16[512,2048]{1,0:T(8,128)(2,1)}, u32[]{:S(2)}) copy-start(bf16[512,2048]{1,0:T(8,128)(2,1)} %param.30) | copy-start | bytes 6291460
  6.5 152.3 %copy-start.5 = (bf16[256,128]{1,0:T(8,128)(2,1)S(1)}, bf16[256,128]{1,0:T(8,128)(2,1)}, u32[]{:S(2)}) copy-start(bf16[256,128]{1,0:T(8,128)(2,1)} %param.24) | copy-start | bytes 196612
  6.5 233.0 %reduce-scatter.3.cloned.1.call-start = ((), (), s32[]{:S(2)}) async-start(), calls=%async_computation.4 | async-start | bytes 1310720 | tf_op jit(solution)/shard_map/reduce_scatter | solution.py:195
  192.9 0.6 copy-start.15
  195.3 2.6 copy-start.6
  198.0 2.9 copy-start.10
  198.0 3.0 copy-start.3
  198.0 3.0 copy-start.16
  198.0 3.0 copy-start.19
  199.7 1.8 copy-start.12
  202.8 0.5 copy-start.17
  203.4 3.8 copy-start.7
  207.2 2.3 copy-start.11
  207.2 2.4 copy-start.4
  207.2 2.4 copy-start.20
  208.9 1.2 copy-start.13
  214.7 2.7 copy-start.8
  214.7 24.9 %copy-start.1 = (bf16[64,2048]{1,0:T(8,128)(2,1)S(1)}, bf16[64,2048]{1,0:T(8,128)(2,1)}, u32[]{:S(2)}) copy-start(bf16[64,2048]{1,0:T(8,128)(2,1)} %param.21) | copy-start | bytes 786436
  214.7 26.0 %copy-start.9 = (f32[2048]{0:T(1024)S(1)}, f32[2048]{0:T(1024)}, u32[]{:S(2)}) copy-start(f32[2048]{0:T(1024)} %param.32) | copy-start | bytes 24580
  217.3 88.8 %all-gather.2.cloned.1.call-start = ((), (), s32[]{:S(2)}) async-start(), calls=%async_computation.5 | async-start | bytes 5242880 | tf_op jit(solution)/shard_map/all_gather | solution.py:219
  242.1 63.9 %copy-start.18 = (bf16[1,2048,256]{2,1,0:T(8,128)(2,1)S(1)}, bf16[1,2048,256]{2,1,0:T(8,128)(2,1)}, u32[]{:S(2)}) copy-start(bf16[1,2048,256]{2,1,0:T(8,128)(2,1)} %param.35) | copy-start | bytes 3145732
  273.3 91.4 %reduce-scatter.5.cloned.1.call-start = ((), (), s32[]{:S(2)}) async-start(), calls=%async_computation.6 | async-start | bytes 5242880 | tf_op jit(solution)/shard_map/reduce_scatter | solution.py:223
  320.0 50.6 %copy-start.14 = (f32[64,2]{0,1:T(2,128)S(1)}, f32[64,2]{0,1:T(2,128)}, u32[]{:S(2)}) copy-start(f32[64,2]{0,1:T(2,128)} %param.34) | copy-start | bytes 1540
  364.7 31.2 %all-to-all-start.1 = ((bf16[8,32,2048]{2,1,0:T(8,128)(2,1)}), bf16[8,32,2048]{2,1,0:T(8,128)(2,1)S(1)}, u32[]{:S(2)}, u32[]{:S(2)}) async-start(bf16[8,32,2048]{2,1,0:T(8,128)(2,1)} %bitcast.151), calls=%async_computation.3 | async-start | bytes 2097152 | tf_op jit(solution)/shard_map/all_to_all | solution.py:229
  397.6 4.0 copy-start.2
Sparse Core Ops, SparseCore 0:
  217.4 22.1 reduce-scatter.2
  273.5 32.5 all-gather.1
  320.1 44.5 reduce-scatter.4
where the time goes:
time: 410 us; the launch traced here: 409 us
  blocking collectives  208 us (51%)
  waiting for transfers between devices  124 us (30%)
  matrix products  25.6 us (6%)
  other arithmetic  18.2 us (4%)
  local copies, waits for them, and re-layouts  14.4 us (4%)
  between operations  13.4 us (3%)
  starting transfers between devices  5.77 us (1%)
    reduce_scatter x1, waiting for transfers between devices, body(): lax.psum_scatter(jnp.dot(hidden, down_weight[0], preferred_element_type=j...  44.7 us
    all_gather x1, blocking collectives, body(): keys_wide = lax.all_gather(key_wide, 'sp', axis=0, tiled=True)  33.7 us
    all_gather x1, blocking collectives, body(): keys_narrow = lax.all_gather(key_narrow, 'sp', axis=0, tiled=True)  33.5 us
    all_gather x1, waiting for transfers between devices, body(): lax.all_gather(arrived.reshape(-1, features), 'tp', axis=0, tiled=True)  32.5 us
    all_gather x1, blocking collectives, body(): values_narrow = lax.all_gather(value_narrow, 'sp', axis=0, tiled=True)  31.4 us
    all_gather x1, blocking collectives, body(): values_wide = lax.all_gather(value_wide, 'sp', axis=0, tiled=True)  31.2 us
    all_to_all x1, blocking collectives, body(): lax.all_to_all(outgoing, 'sp', split_axis=0, concat_axis=0, tiled=True)  31.1 us
    all_gather x1, blocking collectives, body(): lax.all_gather(running_narrow, 'sp', axis=0, tiled=True)  27.9 us
  transfers between devices with their start and end apart: 4, of which 4 were waited for; matrix products, arithmetic and copies ran while one was open for 0% of the time, Pallas kernels for 0%

commit v1 on v0

--- a/solution.py
+++ b/solution.py
@@ -1,8 +1,11 @@
+import functools
 import math
 
 import jax
 import jax.numpy as jnp
 from jax import lax
+from jax.experimental import pallas as pl
+from jax.experimental.pallas import tpu as pltpu
 from jax.sharding import PartitionSpec as P
 
 HW = 128
@@ -239,6 +242,524 @@
     return (middle_wide + combined).astype(jnp.bfloat16)
 
 
+CORES = 2
+MESH = pl.DeviceIdType.MESH
+VMEM = pl.BlockSpec(memory_space=pltpu.VMEM)
+
+
+def greet(peers):
+    barrier = pltpu.get_barrier_semaphore()
+    for peer in peers:
+        pl.semaphore_signal(barrier, inc=1, device_id=peer, device_id_type=MESH)
+    pl.semaphore_wait(barrier, len(peers))
+
+
+def remote(source, target, send, receive, peer):
+    return pltpu.make_async_remote_copy(
+        src_ref=source,
+        dst_ref=target,
+        send_sem=send,
+        recv_sem=receive,
+        device_id=peer,
+        device_id_type=MESH,
+    )
+
+
+def call(kernel, number, outs, scratch, args):
+    return pl.pallas_call(
+        kernel,
+        out_shape=outs,
+        in_specs=[VMEM] * len(args),
+        out_specs=[VMEM] * len(outs),
+        scratch_shapes=scratch,
+        compiler_params=pltpu.CompilerParams(collective_id=number, has_side_effects=True),
+    )(*args)
+
+
+DMA = pltpu.SemaphoreType.DMA
+
+
+def keys_kernel(outer, inner, count, *refs):
+    ins, outs = refs[:count], refs[count : 2 * count]
+    local, send_up, take_up, send_in, take_in = refs[2 * count :]
+    place = lax.axis_index("sp")
+    o, i = place // inner, place % inner
+    tp = lax.axis_index("tp")
+
+    def at(o_, i_):
+        return (o_ * inner + i_, tp)
+
+    greet(
+        [at((o + d) % outer, i) for d in range(1, outer)]
+        + [at(o, (i + d) % inner) for d in range(1, inner)]
+    )
+    other = at((o + 1) % outer, i)
+
+    def up(t, a):
+        slot = (o - t) * inner + i
+        source = ins[a] if t == 0 else outs[a].at[slot]
+        return remote(source, outs[a].at[slot], send_up.at[t, a], take_up.at[t, a], at(o + 1, i))
+
+    def across(t, d, a):
+        slot = (o - t) * inner + i
+        source = ins[a] if t == 0 else outs[a].at[slot]
+        return remote(
+            source,
+            outs[a].at[slot],
+            send_in.at[t, d - 1, a],
+            take_in.at[t, d - 1, a],
+            at(o, (i + d) % inner),
+        )
+
+    def landed(slot, a, semaphore):
+        remote(outs[a].at[slot], outs[a].at[slot], semaphore, semaphore, other).wait_recv()
+
+    for a in range(count):
+        pltpu.make_async_copy(ins[a], outs[a].at[place], local.at[a]).start()
+    for t in range(outer):
+
+        @pl.when(o >= t)
+        def _(t=t):
+            for a in range(count):
+                if t > 0:
+                    landed((o - t) * inner + i, a, take_up.at[t - 1, a])
+                if t < outer - 1:
+
+                    @pl.when(o + 1 < outer)
+                    def _(a=a):
+                        up(t, a).start()
+
+                for d in range(1, inner):
+                    if t > 0:
+                        across(t, d, a).start()
+                    else:
+
+                        @pl.when((i + d) % inner > i)
+                        def _(a=a, d=d):
+                            across(t, d, a).start()
+
+    for t in range(outer):
+
+        @pl.when(o >= t)
+        def _(t=t):
+            for a in range(count):
+                for d in range(1, inner):
+                    giver = (i - d + inner) % inner
+                    slot = (o - t) * inner + giver
+                    if t > 0:
+                        landed(slot, a, take_in.at[t, d - 1, a])
+                        across(t, d, a).wait_send()
+                    else:
+
+                        @pl.when(giver < i)
+                        def _(a=a, d=d, slot=slot):
+                            landed(slot, a, take_in.at[0, d - 1, a])
+
+                        @pl.when((i + d) % inner > i)
+                        def _(a=a, d=d):
+                            across(0, d, a).wait_send()
+
+                if t < outer - 1:
+
+                    @pl.when(o + 1 < outer)
+                    def _(a=a):
+                        up(t, a).wait_send()
+
+    for a in range(count):
+        pltpu.make_async_copy(ins[a], outs[a].at[place], local.at[a]).wait()
+
+
+def gather_keys(arrays, outer, inner):
+    count = len(arrays)
+    outs = [jax.ShapeDtypeStruct((outer * inner,) + x.shape, x.dtype) for x in arrays]
+    scratch = [
+        DMA((count,)),
+        DMA((outer, count)),
+        DMA((outer, count)),
+        DMA((outer, inner, count)),
+        DMA((outer, inner, count)),
+    ]
+    return call(functools.partial(keys_kernel, outer, inner, count), 1, outs, scratch, arrays)
+
+
+def attend_kernel(qw, qn, near, kw, vw, kn, vn, far, out, top, total, mixed):
+    place = lax.axis_index("sp")
+    rows = qw.shape[0]
+    width = qn.shape[1]
+    heads = 1 + width // HN
+    lanes = lax.broadcasted_iota(jnp.int32, (rows, width), 1) // HN
+
+    def query(h):
+        if h == 0:
+            return qw[...]
+        return jnp.where(lanes == h - 1, qn[...], jnp.zeros_like(qn[...]))
+
+    def block(j, shift, diagonal):
+        for h in range(heads):
+            keys, values = (kw, vw) if h == 0 else (kn, vn)
+            size = HW if h == 0 else HN
+            scores = lax.dot_general(
+                query(h), keys[j], (((1,), (1,)), ((), ())), preferred_element_type=jnp.float32
+            )
+            drop = (near[:, h : h + 1] + shift[h]) - far[j, h : h + 1, :]
+            scores = scores * size ** (-0.5) + drop
+            if diagonal:
+                t = lax.broadcasted_iota(jnp.int32, scores.shape, 0)
+                s = lax.broadcasted_iota(jnp.int32, scores.shape, 1)
+                scores = jnp.where(s <= t, scores, -jnp.inf)
+            peak = jnp.max(scores, axis=1, keepdims=True)
+            if diagonal:
+                weights = jnp.exp(scores - peak)
+                total[h] = jnp.sum(weights, axis=1, keepdims=True)
+                mixed[h] = jnp.dot(
+                    weights.astype(jnp.bfloat16), values[j], preferred_element_type=jnp.float32
+                )
+                top[h] = peak
+            else:
+                before = top[h]
+                peak = jnp.maximum(before, peak)
+                weights = jnp.exp(scores - peak)
+                shrink = jnp.exp(before - peak)
+                total[h] = total[h] * shrink + jnp.sum(weights, axis=1, keepdims=True)
+                mixed[h] = mixed[h] * shrink + jnp.dot(
+                    weights.astype(jnp.bfloat16), values[j], preferred_element_type=jnp.float32
+                )
+                top[h] = peak
+
+    block(place, [jnp.zeros((1, 1), jnp.float32)] * heads, True)
+
+    def step(t, shift):
+        j = place - 1 - t
+        shift = tuple(shift[h] + far[j, h : h + 1, rows - 1 : rows] for h in range(heads))
+        block(j, shift, False)
+        return shift
+
+    lax.fori_loop(0, place, step, tuple(jnp.zeros((1, 1), jnp.float32) for _ in range(heads)))
+    out[:, : qw.shape[1]] = (mixed[0] / total[0]).astype(jnp.bfloat16)
+    narrow = mixed[1] / total[1]
+    for h in range(2, heads):
+        narrow = jnp.where(lanes == h - 1, mixed[h] / total[h], narrow)
+    out[:, qw.shape[1] :] = narrow.astype(jnp.bfloat16)
+
+
+def swap_kernel(axis, n, stride, source, target, local, send, take):
+    sp, tp = lax.axis_index("sp"), lax.axis_index("tp")
+    me = (sp if axis == "sp" else tp) // stride
+    rest = (sp if axis == "sp" else tp) % stride
+
+    def at(k):
+        return (k * stride + rest, tp) if axis == "sp" else (sp, k * stride + rest)
+
+    greet([at((me + d) % n) for d in range(1, n)])
+
+    def copy(d):
+        k = (me + d) % n
+        return remote(source.at[k], target.at[me], send.at[d], take.at[d], at(k))
+
+    for d in range(1, n):
+        copy(d).start()
+    own = pltpu.make_async_copy(source.at[me], target.at[me], local.at[0])
+    own.start()
+    own.wait()
+    for d in range(1, n):
+        slot = target.at[(me - d + n) % n]
+        remote(slot, slot, send.at[d], take.at[d], at((me + d) % n)).wait_recv()
+        copy(d).wait_send()
+
+
+def swap(array, axis, n, stride, number):
+    return call(
+        functools.partial(swap_kernel, axis, n, stride),
+        number,
+        [jax.ShapeDtypeStruct(array.shape, array.dtype)],
+        [DMA((1,)), DMA((n,)), DMA((n,))],
+        [array],
+    )[0]
+
+
+def spread_kernel(outer, inner, ys, count, *refs):
+    ins, outs = refs[:count], refs[count : 2 * count]
+    local, send_a, take_a, send_b, take_b, send_c, take_c = refs[2 * count :]
+    place, tp = lax.axis_index("sp"), lax.axis_index("tp")
+    o, i, y, c = place // inner, place % inner, tp // CORES, tp % CORES
+    steps = [(di, dy) for di in range(inner) for dy in range(ys) if (di, dy) != (0, 0)]
+    mate = (place, y * CORES + 1 - c)
+
+    def beside(di, dy):
+        return (o * inner + (i + di) % inner, (y + dy) % ys * CORES + c)
+
+    def above(d):
+        return ((o + d) % outer * inner + i, tp)
+
+    greet(
+        [above(d) for d in range(1, outer)] + [beside(di, dy) for di, dy in steps] + [mate]
+    )
+
+    def slot(a, core, t, di, dy):
+        return outs[a].at[
+            core, (o - t + outer) % outer, (i - di + inner) % inner, (y - dy + ys) % ys
+        ]
+
+    def first(d, a):
+        return remote(
+            ins[a].at[(o + d) % outer],
+            outs[a].at[c, o, i, y],
+            send_a.at[d, a],
+            take_a.at[d, a],
+            above(d),
+        )
+
+    def second(t, di, dy, a):
+        source = ins[a].at[o] if t == 0 else slot(a, c, t, 0, 0)
+        return remote(
+            source,
+            slot(a, c, t, 0, 0),
+            send_b.at[t, di, dy, a],
+            take_b.at[t, di, dy, a],
+            beside(di, dy),
+        )
+
+    def third(t, di, dy, a):
+        source = ins[a].at[o] if (t, di, dy) == (0, 0, 0) else slot(a, c, t, di, dy)
+        return remote(
+            source, slot(a, c, t, di, dy), send_c.at[t, di, dy, a], take_c.at[t, di, dy, a], mate
+        )
+
+    def landed(where, semaphore):
+        remote(where, where, semaphore, semaphore, mate).wait_recv()
+
+    def relay(t):
+        for di, dy in steps:
+            for a in range(count):
+                landed(slot(a, c, t, di, dy), take_b.at[t, di, dy, a])
+                third(t, di, dy, a).start()
+
+    for d in range(1, outer):
+        for a in range(count):
+            first(d, a).start()
+    for t in range(outer):
+        for a in range(count):
+            if t == 0:
+                pltpu.make_async_copy(ins[a].at[o], slot(a, c, 0, 0, 0), local.at[a]).start()
+            else:
+                landed(slot(a, c, t, 0, 0), take_a.at[t, a])
+            for di, dy in steps:
+                second(t, di, dy, a).start()
+            third(t, 0, 0, a).start()
+        if t > 0:
+            relay(t - 1)
+    relay(outer - 1)
+    for a in range(count):
+        pltpu.make_async_copy(ins[a].at[o], slot(a, c, 0, 0, 0), local.at[a]).wait()
+        for d in range(1, outer):
+            first(d, a).wait_send()
+        for t in range(outer):
+            for di, dy in [(0, 0)] + steps:
+                landed(slot(a, 1 - c, t, di, dy), take_c.at[t, di, dy, a])
+                third(t, di, dy, a).wait_send()
+                if (di, dy) != (0, 0):
+                    second(t, di, dy, a).wait_send()
+
+
+def spread_rows(arrays, outer, inner, ys):
+    count = len(arrays)
+    outs = [
+        jax.ShapeDtypeStruct((CORES, outer, inner, ys) + x.shape[1:], x.dtype) for x in arrays
+    ]
+    wide = DMA((outer, inner, ys, count))
+    scratch = [DMA((count,)), DMA((outer, count)), DMA((outer, count)), wide, wide, wide, wide]
+    return call(
+        functools.partial(spread_kernel, outer, inner, ys, count), 3, outs, scratch, arrays
+    )
+
+
+def mate_kernel(pieces, source, target, send, take):
+    place, tp = lax.axis_index("sp"), lax.axis_index("tp")
+    y, c = tp // CORES, tp % CORES
+    mate = (place, y * CORES + 1 - c)
+    greet([mate])
+
+    def copy(p):
+        return remote(source.at[1 - c, p], target.at[p], send.at[p], take.at[p], mate)
+
+    for p in range(pieces):
+        copy(p).start()
+    for p in range(pieces):
+        copy(p).wait()
+
+
+def plane_kernel(outer, inner, ys, source, target, send, take):
+    place, tp = lax.axis_index("sp"), lax.axis_index("tp")
+    o, i, y, c = place // inner, place % inner, tp // CORES, tp % CORES
+    steps = [(di, dy) for di in range(inner) for dy in range(ys) if (di, dy) != (0, 0)]
+
+    def beside(di, dy):
+        return (o * inner + (i + di) % inner, (y + dy) % ys * CORES + c)
+
+    greet([beside(di, dy) for di, dy in steps])
+
+    def copy(n, k):
+        di, dy = steps[n]
+        return remote(
+            source.at[k, (i + di) % inner, (y + dy) % ys],
+            target.at[n, k],
+            send.at[n, k],
+            take.at[n, k],
+            beside(di, dy),
+        )
+
+    for k in range(outer):
+        for n in range(len(steps)):
+            copy(n, k).start()
+    for k in range(outer):
+        for n in range(len(steps)):
+            copy(n, k).wait()
+
+
+def fast_body(
+    residual,
+    query_wide,
+    key_wide,
+    value_wide,
+    query_narrow,
+    key_narrow,
+    value_narrow,
+    gate_wide,
+    gate_narrow,
+    out_wide,
+    out_narrow,
+    norm_gain,
+    routing,
+    route_weight,
+    gate_weight,
+    up_weight,
+    down_weight,
+):
+    inner = routing.shape[1]
+    places = lax.axis_size("sp")
+    outer = places // inner
+    parts = lax.axis_size("tp")
+    ys = parts // CORES
+    core = lax.axis_index("tp") % CORES
+    y = lax.axis_index("tp") // CORES
+    i = lax.axis_index("sp") % inner
+    own_rows, features = residual.shape
+
+    gates = jnp.concatenate([gate_wide, gate_narrow], axis=1).T
+    running = jnp.cumsum(jax.nn.log_sigmoid(gates), axis=1)
+    heads = gates.shape[0]
+    far = jnp.pad(running, ((0, -heads % 8), (0, 0)))
+    keys_wide, values_wide, keys_narrow, values_narrow, far = gather_keys(
+        [key_wide, value_wide, key_narrow, value_narrow, far], outer, inner
+    )
+    shard_rows, wide = query_wide.shape
+    narrow = query_narrow.shape[1]
+    att = pl.pallas_call(
+        attend_kernel,
+        out_shape=jax.ShapeDtypeStruct((shard_rows, wide + narrow), jnp.bfloat16),
+        in_specs=[VMEM] * 8,
+        out_specs=VMEM,
+        scratch_shapes=[
+            pltpu.VMEM((heads, shard_rows, 1), jnp.float32),
+            pltpu.VMEM((heads, shard_rows, 1), jnp.float32),
+            pltpu.VMEM((heads, shard_rows, wide), jnp.float32),
+        ],
+    )(
+        query_wide,
+        query_narrow,
+        running.T,
+        keys_wide,
+        values_wide,
+        keys_narrow,
+        values_narrow,
+        far,
+    )
+    att = swap(att.reshape(parts, own_rows, wide + narrow), "tp", parts, 1, 2)
+    att_wide = jnp.transpose(att[:, :, :wide], (1, 0, 2)).reshape(own_rows, parts * wide)
+    att_narrow = jnp.transpose(att[:, :, wide:], (1, 0, 2)).reshape(own_rows, parts * narrow)
+    mixed = jnp.dot(att_wide, out_wide, preferred_element_type=jnp.float32)
+    mixed = mixed + jnp.dot(att_narrow, out_narrow, preferred_element_type=jnp.float32)
+    middle = (residual.astype(jnp.float32) + mixed).astype(jnp.bfloat16)
+    middle_wide = middle.astype(jnp.float32)
+    spread = jnp.mean(middle_wide * middle_wide, axis=1, keepdims=True)
+    normed = (middle_wide * lax.rsqrt(spread + epsilon) * norm_gain).astype(jnp.bfloat16)
+
+    capacity = own_rows * GROUPS // places
+    group = routing[:, 0] // inner
+    matches = (group[:, None] == jnp.arange(GROUPS, dtype=jnp.int32)[None, :]).astype(jnp.int32)
+    ranking = jnp.sum((jnp.cumsum(matches, axis=0) - matches) * matches, axis=1)
+    placing = group * capacity + ranking
+    picker = placing[None, :] == jnp.arange(GROUPS * capacity, dtype=jnp.int32)[:, None]
+    of_expert = jnp.sum(
+        jnp.where(
+            (routing % inner)[:, :, None] == jnp.arange(inner, dtype=jnp.int32)[None, None, :],
+            route_weight[:, :, None],
+            0.0,
+        ),
+        axis=1,
+    )
+    slot_weight = jnp.sum(jnp.where(picker[:, :, None], of_expert[None, :, :], 0.0), axis=1)
+    slot_weight = jnp.pad(slot_weight, ((0, 0), (0, -inner % 128)))
+    picker = picker.astype(jnp.bfloat16)
+    outgoing = jnp.dot(picker, normed, preferred_element_type=jnp.float32).astype(jnp.bfloat16)
+    pooled, pooled_weight = spread_rows(
+        [
+            outgoing.reshape(GROUPS, capacity, features),
+            slot_weight.reshape(GROUPS, capacity, slot_weight.shape[1]),
+        ],
+        outer,
+        inner,
+        ys,
+    )
+    pooled = pooled.reshape(-1, features)
+    pooled_weight = pooled_weight.reshape(pooled.shape[0], -1)
+    scale = jnp.where(i == 0, pooled_weight[:, :1], 0.0)
+    for other in range(1, inner):
+        scale = jnp.where(i == other, pooled_weight[:, other : other + 1], scale)
+    gate_value = jnp.dot(pooled, gate_weight[0], preferred_element_type=jnp.float32)
+    up_value = jnp.dot(pooled, up_weight[0], preferred_element_type=jnp.float32)
+    hidden = (jax.nn.silu(gate_value) * up_value).astype(jnp.bfloat16)
+    answers = jnp.dot(hidden, down_weight[0], preferred_element_type=jnp.float32)
+    answers = (answers * scale).astype(jnp.bfloat16)
+    answers = answers.reshape(CORES, outer, inner, ys, capacity, features)
+    half = jax.ShapeDtypeStruct(answers.shape[1:], jnp.bfloat16)
+    arrived = call(
+        functools.partial(mate_kernel, outer),
+        4,
+        [half],
+        [DMA((outer,)), DMA((outer,))],
+        [answers],
+    )[0]
+    own = lax.dynamic_index_in_dim(answers, core, 0, keepdims=False)
+    chip = (own.astype(jnp.float32) + arrived.astype(jnp.float32)).astype(jnp.bfloat16)
+    others = inner * ys - 1
+    arrived = call(
+        functools.partial(plane_kernel, outer, inner, ys),
+        5,
+        [jax.ShapeDtypeStruct((others, outer, capacity, features), jnp.bfloat16)],
+        [DMA((others, outer)), DMA((others, outer))],
+        [chip],
+    )[0]
+    own = lax.dynamic_slice(
+        chip, (0, i, y, 0, 0), (outer, 1, 1, capacity, features)
+    ).reshape(outer, capacity, features)
+    plane = own.astype(jnp.float32) + jnp.sum(arrived.astype(jnp.float32), axis=0)
+    returned = swap(plane.astype(jnp.bfloat16), "sp", outer, inner, 6)
+    combined = jnp.dot(
+        picker.T, returned.reshape(-1, features), preferred_element_type=jnp.float32
+    )
+    return (middle_wide + combined).astype(jnp.bfloat16)
+
+
+def choose(*args):
+    routing, gate_weight = args[12], args[14]
+    experts = gate_weight.shape[0] * lax.axis_size("sp")
+    paired = lax.axis_size("tp") % CORES == 0 and gate_weight.shape[0] == 1
+    if paired and experts == GROUPS * routing.shape[1]:
+        return fast_body(*args)
+    return body(*args)
+
+
 def solution(mesh):
     placed = (
         P(("sp", "tp"), None),
@@ -260,5 +781,5 @@
         P("sp", "tp", None),
     )
     return jax.shard_map(
-        body, mesh=mesh, in_specs=placed, out_specs=P(("sp", "tp"), None), check_vma=False
-    )
+        choose, mesh=mesh, in_specs=placed, out_specs=P(("sp", "tp"), None), check_vma=False
+    )

time: 410 us -> 183 us (0.45)
  blocking collectives: 208 us -> 0 us
  Pallas kernels: 0 us -> 142 us
  waiting for transfers between devices: 124 us -> 0 us
  between operations: 13.4 us -> 0.24 us
  other arithmetic: 18.2 us -> 10.5 us
  starting transfers between devices: 5.77 us -> 0 us
  matrix products: 25.6 us -> 20.2 us
  local copies, waits for them, and re-layouts: 14.4 us -> 9.21 us
    all_gather x6 -> x0, blocking collectives: 177 us -> none  [the longest x1 33.7 us: body(): keys_wide = lax.all_gather(key_wide, 'sp', axis=0, tiled=True)]
    pallas_call x0 -> x7, Pallas kernels: none -> 142 us  [the longest x6 139 us: call(): pl.pallas_call(kernel, out_shape=outs, in_specs=[VMEM] * len(args), out_s...]
    reduce_scatter x2 -> x0, waiting for transfers between devices: 65.9 us -> none  [the longest x1 44.7 us: body(): lax.psum_scatter(jnp.dot(hidden, down_weight[0], preferred_element_type=j...]
    all_gather x1 -> x0, waiting for transfers between devices: 32.5 us -> none  [body(): lax.all_gather(arrived.reshape(-1, features), 'tp', axis=0, tiled=True)]
    all_to_all x1 -> x0, blocking collectives: 31.1 us -> none  [body(): lax.all_to_all(outgoing, 'sp', split_axis=0, concat_axis=0, tiled=True)]
    all_to_all x1 -> x0, waiting for transfers between devices: 25.2 us -> none  [body(): lax.all_to_all(answers.reshape(expert_count, capacity, features), 'sp', s...]
    all_to_all x1 -> x0, starting transfers between devices: 5.51 us -> none  [body(): lax.all_to_all(answers.reshape(expert_count, capacity, features), 'sp', s...]
    dot_general x13 -> x6, matrix products: 25.6 us -> 20.2 us  [the longest x1 9.42 us: fast_body(): jnp.dot(hidden, down_weight[0], preferred_element_type=jnp.float32)]
  transfers between devices with their start and end apart: 4 -> 0, of which waited for: 4 -> 0; matrix products, arithmetic and copies ran while one was open for 0% -> 0% of each run, Pallas kernels for 0% -> 0%
where the time goes in v1:
time: 183 us
  Pallas kernels  142 us (78%)
  matrix products  20.2 us (11%)
  other arithmetic  10.5 us (6%)
  local copies, waits for them, and re-layouts  9.21 us (5%)
    pallas_call x6, Pallas kernels, call(): pl.pallas_call(kernel, out_shape=outs, in_specs=[VMEM] * len(args), out_s...  139 us
    dot_general x1, matrix products, fast_body(): jnp.dot(hidden, down_weight[0], preferred_element_type=jnp.float32)  9.42 us
    dot_general x1, matrix products, fast_body(): jnp.dot(pooled, gate_weight[0], preferred_element_type=jnp.float32)  4.82 us
    unnamed x19, local copies, waits for them, and re-layouts  3.87 us

profile of v1, /device:TPU:0, one launch (start us, length us, event | category | flops | bytes accessed | tf_op | source)
XLA Modules:
  0.0 182.6 jit_solution(4498590993834025368)
XLA Ops:
  0.0 0.0 copy-start
  0.0 0.9 fusion.28
  0.9 0.9 reduce-window.6
  1.8 0.1 slice.28
  1.9 0.1 copy.40
  2.0 0.1 copy.41
  2.1 0.1 broadcast_add_fusion
  2.2 0.1 copy.42
  2.4 0.0 copy-start.2
  2.4 0.1 copy.55
  2.4 0.6 pad.8.clone.refs_4_
  3.1 14.6 %shard_map.163 = (bf16[8,256,128]{2,1,0:T(8,128)(2,1)}, bf16[8,256,128]{2,1,0:T(8,128)(2,1)}, bf16[8,256,128]{2,1,0:T(8,128)(2,1)}, bf16[8,256,128]{2,1,0:T(8,128)(2,1)}, f32[8,8,256]{2,1,0:T(8,128)}) custom-call(bf16[256,128]{1,0:T(8,128)(2,1)} %refs_0_.1, bf16[256,128]{1,0:T(8,128)(2,1)} %refs_1_.1, bf16[256,128]{1,0:T(8,128)(2,1)} %refs_2_.1, ...), custom_call_target="tpu_custom_call" | custom-call | tf_op jit(solution)/shard_map/pallas_call | solution.py:269
  17.6 0.0 copy-done.2
  17.6 3.6 %shard_map.164 = bf16[256,256]{1,0:T(8,128)(2,1)} custom-call(bf16[256,128]{1,0:T(8,128)(2,1)} %qw.1, bf16[256,128]{1,0:T(8,128)(2,1)} %qn.1, f32[256,3]{1,0:T(8,128)} %bitcast.71, bf16[8,256,128]{2,1,0:T(8,128)(2,1)} %get-tuple-element.12.kw, bf16[8,256,128]{2,1,0:T(8,128)(2,1)} %get-tuple-element.13.vw, bf16[8,256,128]{2,1,0:T(8,128)(2,1)} %get-tuple-element.14.kn, ...), custom_call_target="tpu_custom_call" | custom-call | tf_op jit(solution)/shard_map/pallas_call | solution.py:657
  21.2 0.0 copy-start.3
  21.2 5.7 %shard_map.165 = bf16[4,64,256]{2,1,0:T(8,128)(2,1)} custom-call(bf16[4,64,256]{2,1,0:T(8,128)(2,1)} %bitcast.72), custom_call_target="tpu_custom_call" | custom-call | tf_op jit(solution)/shard_map/pallas_call | solution.py:269
  26.9 0.9 slice_bitcast_fusion
  27.8 2.1 %fusion.22 = f32[64,2048]{1,0:T(8,128)S(1)} fusion(bf16[512,2048]{1,0:T(8,128)(2,1)} %param.26, bf16[4,8,8,128]{3,2,1,0:T(8,128)(2,1)S(1)} %get-tuple-element.22), kind=kOutput, calls=%fused_computation.32 | convolution fusion | flops 134217728 | bytes 2686976 | tf_op jit(solution)/shard_map/dot_general | solution.py:680
  29.9 0.0 copy-start.6
  29.9 0.0 copy-start.4
  29.9 0.0 copy-done
  29.9 0.0 copy-done.3
  29.9 0.0 copy-start.5
  30.0 0.6 multiply_reduce_fusion
  30.6 0.0 copy-done.6
  30.6 0.1 fusion.25
  30.7 0.1 reduce_window_sum.28
  30.8 0.2 select_reduce_fusion.1
  31.0 0.0 copy-done.4
  31.0 1.2 convolution_convert_fusion
  32.2 0.1 iota_compare_fusion
  32.3 0.0 copy-done.5
  32.3 0.1 select_reduce_fusion
  32.4 0.1 copy.56
  32.5 0.6 pad.9.clone
  33.2 67.1 %shard_map.166 = (bf16[2,4,2,2,32,2048]{5,4,3,2,1,0:T(8,128)(2,1)}, f32[2,4,2,2,32,128]{5,4,3,2,1,0:T(8,128)}) custom-call(bf16[4,32,2048]{2,1,0:T(8,128)(2,1)} %bitcast.67, f32[4,32,128]{2,1,0:T(8,128)} %bitcast.73), custom_call_target="tpu_custom_call" | custom-call | tf_op jit(solution)/shard_map/pallas_call | solution.py:269
  100.3 2.2 %fusion.34 = (f32[1024,1]{1,0:T(8,128)S(1)}, f32[1024,1]{1,0:T(8,128)}) fusion(f32[1024,128]{1,0:T(8,128)} %bitcast.69), kind=kLoop, calls=%fused_computation.71 | loop fusion | bytes 16384 | tf_op jit(solution)/shard_map/slice | solution.py:716
  102.5 1.2 copy.52
  103.7 0.2 copy.53
  103.9 4.8 %fusion.10 = f32[1024,256]{1,0:T(8,128)} fusion(bf16[1024,2048]{1,0:T(8,128)(2,1)} %bitcast.76, bf16[1,2048,256]{2,1,0:T(8,128)(2,1)} %param.31), kind=kOutput, calls=%fused_computation.18 | convolution fusion | flops 1073741824 | bytes 6291456 | tf_op jit(solution)/shard_map/dot_general | solution.py:719
  108.7 9.4 %multiply_convert_fusion = bf16[1024,2048]{1,0:T(8,128)(2,1)} fusion(f32[1024]{0:T(1024)S(1)} %bitcast.74, bf16[1024,2048]{1,0:T(8,128)(2,1)} %bitcast.77, bf16[1,256,2048]{2,1,0:T(8,128)(2,1)} %param.33, bf16[1,2048,256]{2,1,0:T(8,128)(2,1)} %param.32, f32[1024,256]{1,0:T(8,128)} %fusion.10), kind=kOutput, calls=%fused_computation | convolution fusion | flops 2153250816 | bytes 11538432 | tf_op jit(solution)/shard_map/dot_general | solution.py:722
  118.2 7.8 %shard_map.167 = bf16[4,2,2,32,2048]{4,3,2,1,0:T(8,128)(2,1)} custom-call(bf16[2,4,2,2,32,2048]{5,4,3,2,1,0:T(8,128)(2,1)} %bitcast.65), custom_call_target="tpu_custom_call" | custom-call | tf_op jit(solution)/shard_map/pallas_call | solution.py:269
  126.0 3.0 %fusion = bf16[4,2,2,32,2048]{4,3,0,2,1:T(8,128)(2,1)S(1)} fusion(bf16[4,2,2,32,2048]{4,3,2,1,0:T(8,128)(2,1)} %shard_map.167, bf16[2,4,2,2,32,2048]{5,4,3,2,1,0:T(8,128)(2,1)} %bitcast.66, s32[]{:T(128)S(6)} %select_n.84), kind=kLoop, calls=%fused_computation.2 | loop fusion | flops 4194304 | bytes 6291460 | tf_op jit(solution)/shard_map/convert_element_type | solution.py:734
  129.0 0.0 copy-start.1
  129.0 1.3 copy-done.1
  130.3 1.4 copy.51.source
  131.8 29.4 %shard_map.168 = bf16[3,4,32,2048]{3,2,1,0:T(8,128)(2,1)} custom-call(bf16[4,2,2,32,2048]{4,3,2,1,0:T(8,128)(2,1)} %copy.51.source), custom_call_target="tpu_custom_call" | custom-call | tf_op jit(solution)/shard_map/pallas_call | solution.py:269
  161.2 2.8 %convert_reduce_fusion = f32[4,32,2048]{2,1,0:T(8,128)} fusion(bf16[3,4,32,2048]{3,2,1,0:T(8,128)(2,1)} %shard_map.168), kind=kLoop, calls=%fused_computation.3 | loop fusion | flops 1310720 | bytes 2621440 | tf_op jit(solution)/shard_map/reduce_sum | solution.py:746
  164.0 2.3 %fusion.6.source = bf16[4,32,2048]{2,1,0:T(8,128)(2,1)} fusion(f32[4,32,2048]{2,1,0:T(8,128)} %convert_reduce_fusion, bf16[4,2,2,32,2048]{4,3,0,2,1:T(8,128)(2,1)} %copy-done.1, s32[]{:T(128)S(6)} %select_n.85, s32[]{:T(128)S(6)} %select_n.87), kind=kLoop, calls=%fused_computation.15 | loop fusion | flops 786432 | bytes 2097160 | tf_op jit(solution)/shard_map/convert_element_type | solution.py:747
  166.2 14.4 %shard_map.169 = bf16[4,32,2048]{2,1,0:T(8,128)(2,1)} custom-call(bf16[4,32,2048]{2,1,0:T(8,128)(2,1)} %fusion.6.source), custom_call_target="tpu_custom_call" | custom-call | tf_op jit(solution)/shard_map/pallas_call | solution.py:269
  180.6 2.0 %fusion.4 = bf16[64,2048]{1,0:T(8,128)(2,1)} fusion(f32[64,2048]{1,0:T(8,128)S(1)} %get-tuple-element.24, bf16[128,2048]{1,0:T(8,128)(2,1)} %bitcast.68, s32[64]{0:T(128)S(1)} %multiply_add_fusion), kind=kOutput, calls=%fused_computation.10 | convolution fusion | flops 33824768 | bytes 1310976 | tf_op jit(solution)/shard_map/dot_general | solution.py:748
  (9 shorter events, 0.1 us)
Async XLA Ops:
  0.0 29.9 %copy-start = (bf16[512,2048]{1,0:T(8,128)(2,1)S(1)}, bf16[512,2048]{1,0:T(8,128)(2,1)}, u32[]{:S(2)}) copy-start(bf16[512,2048]{1,0:T(8,128)(2,1)} %param.27) | copy-start | bytes 6291460
  2.4 15.3 %copy-start.2 = (f32[3,2,128]{0,2,1:T(8,128)}, f32[3,2,128]{0,2,1:T(8,128)S(1)}, u32[]{:S(2)}) copy-start(f32[3,2,128]{0,2,1:T(8,128)S(1)} %copy.42) | copy-start | bytes 9220
  21.2 8.7 %copy-start.3 = (bf16[64,2048]{1,0:T(8,128)(2,1)S(1)}, bf16[64,2048]{1,0:T(8,128)(2,1)}, u32[]{:S(2)}) copy-start(bf16[64,2048]{1,0:T(8,128)(2,1)} %param.17) | copy-start | bytes 786436
  29.9 0.7 copy-start.6
  29.9 1.1 copy-start.4
  29.9 2.4 %copy-start.5 = (f32[64,2]{0,1:T(2,128)S(1)}, f32[64,2]{0,1:T(2,128)}, u32[]{:S(2)}) copy-start(f32[64,2]{0,1:T(2,128)} %param.30) | copy-start | bytes 1540
  129.0 1.4 copy-start.1

commit v2 on v1

--- a/solution.py
+++ b/solution.py
@@ -543,7 +543,7 @@
                 pltpu.make_async_copy(ins[a].at[o], slot(a, c, 0, 0, 0), local.at[a]).start()
             else:
                 landed(slot(a, c, t, 0, 0), take_a.at[t, a])
-            for di, dy in steps:
+            for di, dy in reversed(steps):
                 second(t, di, dy, a).start()
             third(t, 0, 0, a).start()
         if t > 0:
@@ -609,7 +609,7 @@
         )
 
     for k in range(outer):
-        for n in range(len(steps)):
+        for n in reversed(range(len(steps))):
             copy(n, k).start()
     for k in range(outer):
         for n in range(len(steps)):

time: 183 us -> 183 us (level)
  no operation moved by 1% of the time
where the time goes in v2:
time: 183 us; the launch traced here: 182 us
  Pallas kernels  142 us (78%)
  matrix products  20.2 us (11%)
  other arithmetic  10.5 us (6%)
  local copies, waits for them, and re-layouts  9.21 us (5%)
    pallas_call x6, Pallas kernels, call(): pl.pallas_call(kernel, out_shape=outs, in_specs=[VMEM] * len(args), out_s...  138 us
    dot_general x1, matrix products, fast_body(): jnp.dot(hidden, down_weight[0], preferred_element_type=jnp.float32)  9.42 us
    dot_general x1, matrix products, fast_body(): jnp.dot(pooled, gate_weight[0], preferred_element_type=jnp.float32)  4.82 us
    unnamed x19, local copies, waits for them, and re-layouts  3.87 us

profile of v2, /device:TPU:0, one launch (start us, length us, event | category | flops | bytes accessed | tf_op | source)
XLA Modules:
  0.0 181.9 jit_solution(697721297730779662)
XLA Ops:
  0.0 0.0 copy-start
  0.0 0.9 fusion.28
  0.9 0.9 reduce-window.6
  1.8 0.1 slice.28
  1.9 0.1 copy.40
  2.0 0.1 copy.41
  2.1 0.1 broadcast_add_fusion
  2.2 0.1 copy.42
  2.4 0.0 copy-start.2
  2.4 0.1 copy.55
  2.4 0.6 pad.8.clone.refs_4_
  3.1 14.6 %shard_map.163 = (bf16[8,256,128]{2,1,0:T(8,128)(2,1)}, bf16[8,256,128]{2,1,0:T(8,128)(2,1)}, bf16[8,256,128]{2,1,0:T(8,128)(2,1)}, bf16[8,256,128]{2,1,0:T(8,128)(2,1)}, f32[8,8,256]{2,1,0:T(8,128)}) custom-call(bf16[256,128]{1,0:T(8,128)(2,1)} %refs_0_.1, bf16[256,128]{1,0:T(8,128)(2,1)} %refs_1_.1, bf16[256,128]{1,0:T(8,128)(2,1)} %refs_2_.1, ...), custom_call_target="tpu_custom_call" | custom-call | tf_op jit(solution)/shard_map/pallas_call | solution.py:269
  17.6 0.0 copy-done.2
  17.6 3.6 %shard_map.164 = bf16[256,256]{1,0:T(8,128)(2,1)} custom-call(bf16[256,128]{1,0:T(8,128)(2,1)} %qw.1, bf16[256,128]{1,0:T(8,128)(2,1)} %qn.1, f32[256,3]{1,0:T(8,128)} %bitcast.71, bf16[8,256,128]{2,1,0:T(8,128)(2,1)} %get-tuple-element.12.kw, bf16[8,256,128]{2,1,0:T(8,128)(2,1)} %get-tuple-element.13.vw, bf16[8,256,128]{2,1,0:T(8,128)(2,1)} %get-tuple-element.14.kn, ...), custom_call_target="tpu_custom_call" | custom-call | tf_op jit(solution)/shard_map/pallas_call | solution.py:657
  21.2 0.0 copy-start.3
  21.2 5.7 %shard_map.165 = bf16[4,64,256]{2,1,0:T(8,128)(2,1)} custom-call(bf16[4,64,256]{2,1,0:T(8,128)(2,1)} %bitcast.72), custom_call_target="tpu_custom_call" | custom-call | tf_op jit(solution)/shard_map/pallas_call | solution.py:269
  26.9 0.9 slice_bitcast_fusion
  27.8 2.1 %fusion.22 = f32[64,2048]{1,0:T(8,128)S(1)} fusion(bf16[512,2048]{1,0:T(8,128)(2,1)} %param.26, bf16[4,8,8,128]{3,2,1,0:T(8,128)(2,1)S(1)} %get-tuple-element.22), kind=kOutput, calls=%fused_computation.32 | convolution fusion | flops 134217728 | bytes 2686976 | tf_op jit(solution)/shard_map/dot_general | solution.py:680
  29.9 0.0 copy-start.6
  29.9 0.0 copy-start.4
  29.9 0.0 copy-done
  29.9 0.0 copy-done.3
  29.9 0.0 copy-start.5
  30.0 0.6 multiply_reduce_fusion
  30.6 0.0 copy-done.6
  30.6 0.1 fusion.25
  30.7 0.1 reduce_window_sum.28
  30.8 0.2 select_reduce_fusion.1
  31.0 0.0 copy-done.4
  31.0 1.2 convolution_convert_fusion
  32.2 0.1 iota_compare_fusion
  32.3 0.0 copy-done.5
  32.3 0.1 select_reduce_fusion
  32.4 0.1 copy.56
  32.5 0.6 pad.9.clone
  33.2 66.8 %shard_map.166 = (bf16[2,4,2,2,32,2048]{5,4,3,2,1,0:T(8,128)(2,1)}, f32[2,4,2,2,32,128]{5,4,3,2,1,0:T(8,128)}) custom-call(bf16[4,32,2048]{2,1,0:T(8,128)(2,1)} %bitcast.67, f32[4,32,128]{2,1,0:T(8,128)} %bitcast.73), custom_call_target="tpu_custom_call" | custom-call | tf_op jit(solution)/shard_map/pallas_call | solution.py:269
  100.0 2.2 %fusion.34 = (f32[1024,1]{1,0:T(8,128)S(1)}, f32[1024,1]{1,0:T(8,128)}) fusion(f32[1024,128]{1,0:T(8,128)} %bitcast.69), kind=kLoop, calls=%fused_computation.71 | loop fusion | bytes 16384 | tf_op jit(solution)/shard_map/slice | solution.py:716
  102.2 1.2 copy.52
  103.4 0.2 copy.53
  103.6 4.8 %fusion.10 = f32[1024,256]{1,0:T(8,128)} fusion(bf16[1024,2048]{1,0:T(8,128)(2,1)} %bitcast.76, bf16[1,2048,256]{2,1,0:T(8,128)(2,1)} %param.31), kind=kOutput, calls=%fused_computation.18 | convolution fusion | flops 1073741824 | bytes 6291456 | tf_op jit(solution)/shard_map/dot_general | solution.py:719
  108.4 9.4 %multiply_convert_fusion = bf16[1024,2048]{1,0:T(8,128)(2,1)} fusion(f32[1024]{0:T(1024)S(1)} %bitcast.74, bf16[1024,2048]{1,0:T(8,128)(2,1)} %bitcast.77, bf16[1,256,2048]{2,1,0:T(8,128)(2,1)} %param.33, bf16[1,2048,256]{2,1,0:T(8,128)(2,1)} %param.32, f32[1024,256]{1,0:T(8,128)} %fusion.10), kind=kOutput, calls=%fused_computation | convolution fusion | flops 2153250816 | bytes 11538432 | tf_op jit(solution)/shard_map/dot_general | solution.py:722
  117.8 7.8 %shard_map.167 = bf16[4,2,2,32,2048]{4,3,2,1,0:T(8,128)(2,1)} custom-call(bf16[2,4,2,2,32,2048]{5,4,3,2,1,0:T(8,128)(2,1)} %bitcast.65), custom_call_target="tpu_custom_call" | custom-call | tf_op jit(solution)/shard_map/pallas_call | solution.py:269
  125.6 3.0 %fusion = bf16[4,2,2,32,2048]{4,3,0,2,1:T(8,128)(2,1)S(1)} fusion(bf16[4,2,2,32,2048]{4,3,2,1,0:T(8,128)(2,1)} %shard_map.167, bf16[2,4,2,2,32,2048]{5,4,3,2,1,0:T(8,128)(2,1)} %bitcast.66, s32[]{:T(128)S(6)} %select_n.84), kind=kLoop, calls=%fused_computation.2 | loop fusion | flops 4194304 | bytes 6291460 | tf_op jit(solution)/shard_map/convert_element_type | solution.py:734
  128.7 0.0 copy-start.1
  128.7 1.3 copy-done.1
  130.0 1.4 copy.51.source
  131.4 29.0 %shard_map.168 = bf16[3,4,32,2048]{3,2,1,0:T(8,128)(2,1)} custom-call(bf16[4,2,2,32,2048]{4,3,2,1,0:T(8,128)(2,1)} %copy.51.source), custom_call_target="tpu_custom_call" | custom-call | tf_op jit(solution)/shard_map/pallas_call | solution.py:269
  160.4 2.8 %convert_reduce_fusion = f32[4,32,2048]{2,1,0:T(8,128)} fusion(bf16[3,4,32,2048]{3,2,1,0:T(8,128)(2,1)} %shard_map.168), kind=kLoop, calls=%fused_computation.3 | loop fusion | flops 1310720 | bytes 2621440 | tf_op jit(solution)/shard_map/reduce_sum | solution.py:746
  163.2 2.3 %fusion.6.source = bf16[4,32,2048]{2,1,0:T(8,128)(2,1)} fusion(f32[4,32,2048]{2,1,0:T(8,128)} %convert_reduce_fusion, bf16[4,2,2,32,2048]{4,3,0,2,1:T(8,128)(2,1)} %copy-done.1, s32[]{:T(128)S(6)} %select_n.85, s32[]{:T(128)S(6)} %select_n.87), kind=kLoop, calls=%fused_computation.15 | loop fusion | flops 786432 | bytes 2097160 | tf_op jit(solution)/shard_map/convert_element_type | solution.py:747
  165.5 14.4 %shard_map.169 = bf16[4,32,2048]{2,1,0:T(8,128)(2,1)} custom-call(bf16[4,32,2048]{2,1,0:T(8,128)(2,1)} %fusion.6.source), custom_call_target="tpu_custom_call" | custom-call | tf_op jit(solution)/shard_map/pallas_call | solution.py:269
  179.9 2.0 %fusion.4 = bf16[64,2048]{1,0:T(8,128)(2,1)} fusion(f32[64,2048]{1,0:T(8,128)S(1)} %get-tuple-element.24, bf16[128,2048]{1,0:T(8,128)(2,1)} %bitcast.68, s32[64]{0:T(128)S(1)} %multiply_add_fusion), kind=kOutput, calls=%fused_computation.10 | convolution fusion | flops 33824768 | bytes 1310976 | tf_op jit(solution)/shard_map/dot_general | solution.py:748
  (9 shorter events, 0.1 us)
Async XLA Ops:
  0.0 29.9 %copy-start = (bf16[512,2048]{1,0:T(8,128)(2,1)S(1)}, bf16[512,2048]{1,0:T(8,128)(2,1)}, u32[]{:S(2)}) copy-start(bf16[512,2048]{1,0:T(8,128)(2,1)} %param.27) | copy-start | bytes 6291460
  2.4 15.3 %copy-start.2 = (f32[3,2,128]{0,2,1:T(8,128)}, f32[3,2,128]{0,2,1:T(8,128)S(1)}, u32[]{:S(2)}) copy-start(f32[3,2,128]{0,2,1:T(8,128)S(1)} %copy.42) | copy-start | bytes 9220
  21.2 8.7 %copy-start.3 = (bf16[64,2048]{1,0:T(8,128)(2,1)S(1)}, bf16[64,2048]{1,0:T(8,128)(2,1)}, u32[]{:S(2)}) copy-start(bf16[64,2048]{1,0:T(8,128)(2,1)} %param.17) | copy-start | bytes 786436
  29.9 0.7 copy-start.6
  29.9 1.1 copy-start.4
  29.9 2.4 %copy-start.5 = (f32[64,2]{0,1:T(2,128)S(1)}, f32[64,2]{0,1:T(2,128)}, u32[]{:S(2)}) copy-start(f32[64,2]{0,1:T(2,128)} %param.30) | copy-start | bytes 1540
  128.7 1.4 copy-start.1
